TPU v7x, 32 devices: a whole 2x2x4 slice. The times are simulated.
32 devices in a mesh: ep: 8 (over z, x), tp: 4 (over y, core).
Axes of the slice: x: 2, y: 2, z: 4, core: 2. Of those that a mesh axis runs over, the one named last changes fastest.
Arguments:
- mix_bgate: bfloat16 [2048, 1024], P('ep', 'tp'), may hold values from -6 to 6
- mix_cgate: bfloat16 [2048, 1024], P('ep', 'tp'), may hold values from -6 to 6
- mix_input: bfloat16 [2048, 1024], P('ep', 'tp'), may hold values from -6 to 6
- conv_taps: float32 [3, 1024], P(None, 'tp'), may hold values from -3.5 to 3.5
- mix_out_w: bfloat16 [1024, 2048], P('tp'), may hold values from -0.1875 to 0.1875
- moe_x: bfloat16 [2048, 2048], P('ep', 'tp'), may hold values from -6 to 6
- moe_gain: float32 [2048], replicated, may hold values from 0.1 to 1.9
- routes: int32 [2048, 2], P('ep'), may hold values from 0 to 7, all different within a row; in each aligned block of 256 rows (0 to 255, 256 to 511, ...) at most 96 rows name the same one
- route_w: float32 [2048, 2], P('ep'), may hold values from 0.2 to 1
- w_gate: bfloat16 [8, 2048, 3584], P('ep', None, 'tp'), may hold values from -0.125 to 0.125
- w_up: bfloat16 [8, 2048, 3584], P('ep', None, 'tp'), may hold values from -0.125 to 0.125
- w_down: bfloat16 [8, 3584, 2048], P('ep', 'tp'), may hold values from -0.09375 to 0.09375
Outputs:
- mixed: bfloat16 [2048, 2048], P(('ep', 'tp'))
- routed: bfloat16 [2048, 2048], P('ep', 'tp')
Inputs may be any that keep to these rules, and one draw needn't show every extreme that they name: `routes`: among the 256 rows of one index of ep, each row names 2 different experts and no expert is named by more than 96 rows; in every draw some expert is named by exactly 96 rows of some index.
All inputs are finite; a program needn't handle non-finite values.
Results may differ from a plain program's by a relative error of at most 0.012.
Values may be sent and summed in bfloat16 or wider, within the bound.
A program may use at most 64 MiB of HBM per device.

v0:
```python
import jax
import jax.numpy as jnp
from jax import lax
from jax.sharding import PartitionSpec as P


def shifted(block, axis, distance):
    devices = range(lax.axis_size(axis))
    route = [(i - distance, i) for i in devices if i - distance in devices]
    return lax.ppermute(block, axis, route)


def rms_rows(values, gain):
    wide = values.astype(jnp.float32)
    scale = lax.rsqrt(jnp.mean(wide * wide, axis=-1, keepdims=True) + 1e-06)
    return (wide * scale * gain).astype(jnp.bfloat16)


def conv_mixer(mix_bgate, mix_cgate, mix_input, conv_taps, mix_out_w):
    length = mix_input.shape[0]
    reach = conv_taps.shape[0] - 1
    tail = jnp.stack([mix_cgate[length - reach :], mix_input[length - reach :]])
    before = shifted(tail, "ep", 1)
    gates_c = jnp.concatenate([before[0], mix_cgate], 0).astype(jnp.float32)
    inputs_h = jnp.concatenate([before[1], mix_input], 0).astype(jnp.float32)
    prod = gates_c * inputs_h
    conv = conv_taps[0] * prod[0:length]
    for j in range(1, reach + 1):
        conv = conv + conv_taps[j] * prod[j : j + length]
    gated = (mix_bgate.astype(jnp.float32) * conv).astype(jnp.bfloat16)
    return lax.psum_scatter(
        jnp.dot(gated, mix_out_w, preferred_element_type=jnp.float32).astype(jnp.bfloat16),
        "tp",
        scatter_dimension=0,
        tiled=True,
    )


def expert_layer(moe_x, moe_gain, routes, route_w, w_gate, w_up, w_down):
    whole = lax.all_gather(moe_x, "tp", axis=1, tiled=True)
    normed = rms_rows(whole, moe_gain)
    ntok, width = normed.shape
    top = routes.shape[1]
    n_ep = lax.axis_size("ep")
    n_tp = lax.axis_size("tp")
    per_dev = w_gate.shape[0]
    experts = per_dev * n_ep
    cap = 4 * ((3 * ntok * top + 8 * experts - 1) // (8 * experts))
    flat = routes.reshape(-1)
    onehot = (flat[:, None] == jnp.arange(experts, dtype=jnp.int32)[None, :]).astype(jnp.int32)
    earlier = jnp.cumsum(onehot, axis=0) - onehot
    slot = jnp.sum(earlier * onehot, axis=1)
    place = flat * cap + slot
    source = (
        jnp.full((experts * cap,), ntok, jnp.int32)
        .at[place]
        .set(jnp.arange(ntok * top, dtype=jnp.int32) // top)
    )
    padded = jnp.concatenate([normed, jnp.zeros((1, width), jnp.bfloat16)], 0)
    outgoing = padded[source].reshape(n_ep, per_dev, cap, width)
    part = cap // n_tp
    mine = lax.dynamic_slice_in_dim(outgoing, lax.axis_index("tp") * part, part, 2)
    landed = lax.all_to_all(mine, "ep", split_axis=0, concat_axis=0, tiled=True)
    arrived = lax.all_gather(landed, "tp", axis=2, tiled=True)
    gate = jnp.einsum("secd,edf->secf", arrived, w_gate, preferred_element_type=jnp.float32)
    upper = jnp.einsum("secd,edf->secf", arrived, w_up, preferred_element_type=jnp.float32)
    hidden = (jax.nn.silu(gate) * upper).astype(jnp.bfloat16)
    down = jnp.einsum("secf,efd->secd", hidden, w_down, preferred_element_type=jnp.float32)
    summed = lax.psum_scatter(down.astype(jnp.bfloat16), "tp", scatter_dimension=3, tiled=True)
    returned = lax.all_to_all(summed, "ep", split_axis=0, concat_axis=0, tiled=True)
    flat_back = returned.reshape(experts * cap, width // n_tp)
    picked = flat_back[place].astype(jnp.float32).reshape(ntok, top, width // n_tp)
    return jnp.sum(picked * route_w[:, :, None], axis=1).astype(jnp.bfloat16)


def body(
    mix_bgate,
    mix_cgate,
    mix_input,
    conv_taps,
    mix_out_w,
    moe_x,
    moe_gain,
    routes,
    route_w,
    w_gate,
    w_up,
    w_down,
):
    mixed = conv_mixer(mix_bgate, mix_cgate, mix_input, conv_taps, mix_out_w)
    routed = expert_layer(moe_x, moe_gain, routes, route_w, w_gate, w_up, w_down)
    return (mixed, routed)


def solution(mesh):
    in_specs = (
        P("ep", "tp"),
        P("ep", "tp"),
        P("ep", "tp"),
        P(None, "tp"),
        P("tp", None),
        P("ep", "tp"),
        P(),
        P("ep", None),
        P("ep", None),
        P("ep", None, "tp"),
        P("ep", None, "tp"),
        P("ep", "tp", None),
    )
    out_specs = (P(("ep", "tp"), None), P("ep", "tp"))
    return jax.shard_map(body, mesh=mesh, in_specs=in_specs, out_specs=out_specs, check_vma=False)
```

profile of v0, /device:TPU:0, one launch (start us, length us, event | category | flops | bytes accessed | tf_op | source)
XLA Modules:
  0.0 185.2 jit_solution(3375936974495529147)
XLA Ops:
  7.2 0.0 copy-start
  7.2 0.0 all-gather.3.cloned.1.call-start
  7.2 0.7 all-gather.3.cloned.1.call-update
  7.9 0.0 all-gather.5.cloned.1.call-start
  8.0 0.8 copy.20
  8.8 0.1 eq.29
  8.9 0.1 eq.25
  9.1 1.1 reduce-window.6
  10.2 0.2 slice_reduce_fusion
  10.5 0.7 broadcast_multiply_fusion
  11.2 0.1 copy.19
  11.3 0.1 mul.110
  11.5 0.1 fusion.43
  11.6 2.4 %scatter_custom_fusion = s32[768]{0:T(1024)S(1)} fusion(s32[512]{0:T(512)S(1)} %bitcast.108, s32[512]{0:T(512)S(1)} %add_select_fusion, s32[]{:T(128)} %constant.40.clone.1), kind=kCustom, calls=%fused_computation.57 | custom fusion | bytes 3076 | tf_op jit(solution)/shard_map/scatter | solution.py:57
  14.1 15.0 %all-gather.3.cloned.1.call-done = bf16[256,2048]{1,0:T(8,128)(2,1)} async-done(((bf16[256,512]{1,0:T(8,128)(2,1)}), bf16[256,2048]{1,0:T(8,128)(2,1)}) %all-gather.3.cloned.1.call-update) | async-done | bytes 1048592 | tf_op jit(solution)/shard_map/all_gather | solution.py:40
  29.0 1.5 fusion.18
  30.6 1.5 fusion.20
  32.1 0.1 concatenate.11
  32.2 4.3 %gather_fusion = bf16[768,2048]{1,0:T(8,128)(2,1)} fusion(bf16[257,2048]{1,0:T(8,128)(2,1)S(1)} %concatenate.11, s32[1024]{0:T(1024)S(1)} %pad_clamp_fusion.1), kind=kCustom, calls=%fused_computation | custom fusion | bytes 6294528 | tf_op jit(solution)/shard_map/gather | solution.py:60
  36.5 1.2 constant_dynamic-slice_fusion
  37.7 25.9 %all_to_all.10 = bf16[8,1,24,2048]{3,2,1,0:T(8,128)(2,1)} all-to-all(bf16[8,1,24,2048]{3,2,1,0:T(8,128)(2,1)S(1)} %constant_dynamic-slice_fusion), channel_id=1, replica_groups=mesh['ep'=8,'tp'=4] {'ep'}, dimensions={0} | all-to-all | bytes 1572864 | tf_op jit(solution)/shard_map/all_to_all | solution.py:63
  63.6 0.0 all-gather.5.cloned.1.call-update
  63.6 0.0 reduce-scatter.5.cloned.1.call-start
  63.7 26.7 %all-gather.5.cloned.1.call-done = bf16[8,1,96,2048]{3,2,0,1:T(8,128)(2,1)} async-done(((bf16[8,1,24,2048]{3,2,0,1:T(8,128)(2,1)}), bf16[8,1,96,2048]{3,2,0,1:T(8,128)(2,1)}) %all-gather.5.cloned.1.call-update) | async-done | bytes 3145744 | tf_op jit(solution)/shard_map/all_gather | solution.py:64
  90.4 8.0 %fusion.4 = f32[8,96,896]{2,1,0:T(8,128)} fusion(bf16[1,2048,896]{2,1,0:T(8,128)(2,1)} %param.21, bf16[8,1,96,2048]{3,2,0,1:T(8,128)(2,1)} %all-gather.5.cloned.1.call-done), kind=kOutput, calls=%fused_computation.7 | convolution fusion | flops 2818572288 | bytes 9568256 | tf_op jit(solution)/shard_map/secd,edf->secf/dot_general | solution.py:65
  98.4 12.1 %fusion.11 = bf16[8,1,96,2048]{3,2,0,1:T(8,128)(2,1)} fusion(bf16[1,896,2048]{2,1,0:T(8,128)(2,1)} %param.23, bf16[1,2048,896]{2,1,0:T(8,128)(2,1)} %param.22, bf16[8,1,96,2048]{3,2,0,1:T(8,128)(2,1)} %all-gather.5.cloned.1.call-done, f32[8,96,896]{2,1,0:T(8,128)} %fusion.4), kind=kOutput, calls=%fused_computation.12 | convolution fusion | flops 5642846208 | bytes 16384000 | tf_op jit(solution)/shard_map/secf,efd->secd/dot_general | solution.py:68
  110.5 0.0 copy-start.1
  110.5 0.0 copy-start.2
  110.5 0.0 copy-start.4
  110.5 0.0 copy-start.3
  110.5 0.0 reduce-scatter.5.cloned.1.call-update
  110.5 0.0 copy-start.5
  110.5 0.0 reduce-scatter.3.cloned.1.call-start
  110.6 0.8 copy-done.1
  111.4 0.1 copy-done.2
  111.5 3.4 %collective-permute-start = (bf16[2,2,256]{2,1,0:T(2,128)(2,1)S(1)}, bf16[2,2,256]{2,1,0:T(2,128)(2,1)S(1)}, u32[]{:S(2)}, u32[]{:S(2)}) collective-permute-start(bf16[2,2,256]{2,1,0:T(2,128)(2,1)S(1)} %pad_maximum_fusion), channel_id=1, source_target_pairs={{0,4},{4,8},{8,12},{12,16},{16,20},{20,24},{24,28},{1,5},{5,9},{9,... | collective-permute-start | bytes 6152 | tf_op jit(solution)/shard_map/ppermute | solution.py:10
  114.9 0.0 copy-done.4
  114.9 1.3 collective-permute-done
  116.2 0.1 convert_multiply_fusion.2
  116.2 0.0 copy-done
  116.2 0.0 copy-done.3
  116.2 1.5 convolution_convert_fusion
  117.7 0.0 reduce-scatter.3.cloned.1.call-update
  117.7 30.7 %reduce-scatter.5.cloned.1.call-done = bf16[8,1,96,512]{3,2,0,1:T(8,128)(2,1)} async-done(((bf16[8,1,96,2048]{3,2,0,1:T(8,128)(2,1)}), bf16[8,1,96,512]{3,2,0,1:T(8,128)(2,1)}) %reduce-scatter.5.cloned.1.call-update) | async-done | bytes 786448 | tf_op jit(solution)/shard_map/reduce_scatter | solution.py:69
  148.4 5.5 %all-to-all-start.1 = ((bf16[8,1,96,512]{3,2,1,0:T(8,128)(2,1)}), bf16[8,1,96,512]{3,2,1,0:T(8,128)(2,1)S(1)}, u32[]{:S(2)}, u32[]{:S(2)}) async-start(bf16[8,1,96,512]{3,2,1,0:T(8,128)(2,1)} %bitcast.107), calls=%async_computation.3 | async-start | bytes 1572864 | tf_op jit(solution)/shard_map/all_to_all | solution.py:70
  153.9 0.0 copy-done.5
  153.9 0.1 copy.25
  154.1 19.9 %all-to-all-done.1 = bf16[8,1,96,512]{3,2,1,0:T(8,128)(2,1)S(1)} async-done(((bf16[8,1,96,512]{3,2,1,0:T(8,128)(2,1)}), bf16[8,1,96,512]{3,2,1,0:T(8,128)(2,1)S(1)}, u32[]{:S(2)}, u32[]{:S(2)}) %all-to-all-start.1) | async-done | bytes 786464 | tf_op jit(solution)/shard_map/all_to_all | solution.py:70
  174.0 2.0 %gather_fusion.1 = bf16[512,512]{1,0:T(8,128)(2,1)S(1)} fusion(bf16[768,512]{1,0:T(8,128)(2,1)S(1)} %bitcast.104, s32[1024]{0:T(1024)S(1)} %pad_clamp_fusion), kind=kCustom, calls=%fused_computation.1 | custom fusion | bytes 1050624 | tf_op jit(solution)/shard_map/gather | solution.py:72
  176.0 0.7 reshape.98
  176.6 2.1 %multiply_reduce_fusion = bf16[256,512]{1,0:T(8,128)(2,1)} fusion(f32[256,2,512]{2,1,0:T(2,128)S(1)} %reshape.98, f32[256,2]{1,0:T(8,128)S(1)} %copy.25), kind=kLoop, calls=%fused_computation.27 | loop fusion | flops 393216 | bytes 1312768 | tf_op jit(solution)/shard_map/reduce_sum | solution.py:73
  178.7 0.0 reduce-scatter.3.cloned.1.call-done
  (13 shorter events, 0.1 us)
Async XLA Ops:
  7.2 109.1 %copy-start = (bf16[256,2048]{1,0:T(8,128)(2,1)S(1)}, bf16[256,2048]{1,0:T(8,128)(2,1)}, u32[]{:S(2)}) copy-start(bf16[256,2048]{1,0:T(8,128)(2,1)} %param.16) | copy-start | bytes 3145732
  7.2 21.9 %all-gather.3.cloned.1.call-start = ((), (), s32[]{:S(2)}) async-start(), calls=%async_computation.5 | async-start | bytes 1310720 | tf_op jit(solution)/shard_map/all_gather | solution.py:40
  7.9 82.5 %all-gather.5.cloned.1.call-start = ((), (), s32[]{:S(2)}) async-start(), calls=%async_computation.6 | async-start | bytes 3932160 | tf_op jit(solution)/shard_map/all_gather | solution.py:64
  63.6 84.8 %reduce-scatter.5.cloned.1.call-start = ((), (), s32[]{:S(2)}) async-start(), calls=%async_computation.7 | async-start | bytes 3932160 | tf_op jit(solution)/shard_map/reduce_scatter | solution.py:69
  110.5 0.9 copy-start.1
  110.5 1.0 copy-start.2
  110.5 4.4 %copy-start.4 = (f32[3,256]{1,0:T(4,128)S(1)}, f32[3,256]{1,0:T(4,128)}, u32[]{:S(2)}) copy-start(f32[3,256]{1,0:T(4,128)} %param.15) | copy-start | bytes 9220
  110.5 5.7 %copy-start.3 = (bf16[256,256]{1,0:T(8,128)(2,1)S(1)}, bf16[256,256]{1,0:T(8,128)(2,1)}, u32[]{:S(2)}) copy-start(bf16[256,256]{1,0:T(8,128)(2,1)} %param.12) | copy-start | bytes 393220
  110.5 43.4 %copy-start.5 = (f32[256,2]{0,1:T(2,128)S(1)}, f32[256,2]{0,1:T(2,128)}, u32[]{:S(2)}) copy-start(f32[256,2]{0,1:T(2,128)} %param.20) | copy-start | bytes 6148
  110.5 68.1 %reduce-scatter.3.cloned.1.call-start = ((), (), s32[]{:S(2)}) async-start(), calls=%async_computation.4 | async-start | bytes 1310720 | tf_op jit(solution)/shard_map/reduce_scatter | solution.py:31
  111.5 4.7 %collective-permute-start = (bf16[2,2,256]{2,1,0:T(2,128)(2,1)S(1)}, bf16[2,2,256]{2,1,0:T(2,128)(2,1)S(1)}, u32[]{:S(2)}, u32[]{:S(2)}) collective-permute-start(bf16[2,2,256]{2,1,0:T(2,128)(2,1)S(1)} %pad_maximum_fusion), channel_id=1, source_target_pairs={{0,4},{4,8},{8,12},{12,16},{16,20},{20,24},{24,28},{1,5},{5,9},{9,... | collective-permute-start | bytes 6152 | tf_op jit(solution)/shard_map/ppermute | solution.py:10
  148.4 25.6 %all-to-all-start.1 = ((bf16[8,1,96,512]{3,2,1,0:T(8,128)(2,1)}), bf16[8,1,96,512]{3,2,1,0:T(8,128)(2,1)S(1)}, u32[]{:S(2)}, u32[]{:S(2)}) async-start(bf16[8,1,96,512]{3,2,1,0:T(8,128)(2,1)} %bitcast.107), calls=%async_computation.3 | async-start | bytes 1572864 | tf_op jit(solution)/shard_map/all_to_all | solution.py:70
Sparse Core Ops, SparseCore 0:
  9.5 19.4 all-gather.2
  63.7 26.6 all-gather.4
  110.7 37.7 reduce-scatter.4
  151.4 24.7 reduce-scatter.2
where the time goes:
time: 186 us; the launch traced here: 185 us
  waiting for transfers between devices  94.3 us (51%)
  blocking collectives  25.9 us (14%)
  matrix products  21.5 us (12%)
  between operations  14 us (8%)
  local copies, waits for them, and re-layouts  13.3 us (7%)
  starting transfers between devices  9.05 us (5%)
  other arithmetic  7.18 us (4%)
    reduce_scatter x1, waiting for transfers between devices, expert_layer(): lax.psum_scatter(down.astype(jnp.bfloat16), 'tp', scatter_dimension=3, ti...  30.7 us
    all_gather x1, waiting for transfers between devices, expert_layer(): arrived = lax.all_gather(landed, 'tp', axis=2, tiled=True)  26.7 us
    all_to_all x1, blocking collectives, expert_layer(): landed = lax.all_to_all(mine, 'ep', split_axis=0, concat_axis=0, tiled=True)  25.9 us
    all_to_all x1, waiting for transfers between devices, expert_layer(): lax.all_to_all(summed, 'ep', split_axis=0, concat_axis=0, tiled=True)  19.9 us
    all_gather x1, waiting for transfers between devices, expert_layer(): whole = lax.all_gather(moe_x, 'tp', axis=1, tiled=True)  15 us
    dot_general x1, matrix products, expert_layer(): jnp.einsum('secf,efd->secd', hidden, w_down, preferred_element_type=jnp.f...  12.1 us
    dot_general x1, matrix products, expert_layer(): jnp.einsum('secd,edf->secf', arrived, w_gate, preferred_element_type=jnp....  8 us
    all_to_all x1, starting transfers between devices, expert_layer(): lax.all_to_all(summed, 'ep', split_axis=0, concat_axis=0, tiled=True)  5.52 us
  transfers between devices with their start and end apart: 6, of which 5 were waited for; matrix products, arithmetic and copies ran while one was open for 7% of the time, Pallas kernels for 0%

commit v1 on v0

--- a/solution.py
+++ b/solution.py
@@ -37,7 +37,7 @@
 
 
 def expert_layer(moe_x, moe_gain, routes, route_w, w_gate, w_up, w_down):
-    whole = lax.all_gather(moe_x, "tp", axis=1, tiled=True)
+    whole = jnp.concatenate(lax.all_gather(moe_x, "tp"), axis=1)
     normed = rms_rows(whole, moe_gain)
     ntok, width = normed.shape
     top = routes.shape[1]

time: 186 us -> 187 us (level)
  local copies, waits for them, and re-layouts: 13.3 us -> 15.8 us
where the time goes in v1:
time: 187 us
  waiting for transfers between devices  94.3 us (50%)
  blocking collectives  25.9 us (14%)
  matrix products  21.5 us (11%)
  local copies, waits for them, and re-layouts  15.8 us (8%)
  between operations  14 us (7%)
  starting transfers between devices  9.05 us (5%)
  other arithmetic  6.17 us (3%)
    reduce_scatter x1, waiting for transfers between devices, expert_layer(): lax.psum_scatter(down.astype(jnp.bfloat16), 'tp', scatter_dimension=3, ti...  30.7 us
    all_gather x1, waiting for transfers between devices, expert_layer(): arrived = lax.all_gather(landed, 'tp', axis=2, tiled=True)  26.7 us
    all_to_all x1, blocking collectives, expert_layer(): landed = lax.all_to_all(mine, 'ep', split_axis=0, concat_axis=0, tiled=True)  25.9 us
    all_to_all x1, waiting for transfers between devices, expert_layer(): lax.all_to_all(summed, 'ep', split_axis=0, concat_axis=0, tiled=True)  19.9 us
    all_gather x1, waiting for transfers between devices, expert_layer(): whole = jnp.concatenate(lax.all_gather(moe_x, 'tp'), axis=1)  15 us
    dot_general x1, matrix products, expert_layer(): jnp.einsum('secf,efd->secd', hidden, w_down, preferred_element_type=jnp.f...  12.1 us
    dot_general x1, matrix products, expert_layer(): jnp.einsum('secd,edf->secf', arrived, w_gate, preferred_element_type=jnp....  7.99 us
    all_to_all x1, starting transfers between devices, expert_layer(): lax.all_to_all(summed, 'ep', split_axis=0, concat_axis=0, tiled=True)  5.51 us
  transfers between devices with their start and end apart: 6, of which 5 were waited for; matrix products, arithmetic and copies ran while one was open for 7% of the time, Pallas kernels for 0%

profile of v1, /device:TPU:0, one launch (start us, length us, event | category | flops | bytes accessed | tf_op | source)
XLA Modules:
  0.0 186.8 jit_solution(10500130976953642716)
XLA Ops:
  7.2 0.0 copy-start
  7.2 0.0 all-gather.6.cloned.1.call-start
  7.2 0.7 all-gather.6.cloned.1.call-update
  7.9 0.0 all-gather.4.cloned.1.call-start
  8.0 0.8 copy.23
  8.8 0.1 eq.29
  8.9 0.1 eq.25
  9.1 1.1 reduce-window.6
  10.2 0.2 slice_reduce_fusion
  10.5 0.7 broadcast_multiply_fusion
  11.2 0.1 copy.22
  11.3 0.1 mul.112
  11.5 0.1 fusion.40
  11.6 2.4 %scatter_custom_fusion = s32[768]{0:T(1024)S(1)} fusion(s32[512]{0:T(512)S(1)} %bitcast.117, s32[512]{0:T(512)S(1)} %add_select_fusion, s32[]{:T(128)} %constant.40.clone.1), kind=kCustom, calls=%fused_computation.54 | custom fusion | bytes 3076 | tf_op jit(solution)/shard_map/scatter | solution.py:57
  14.1 15.0 %all-gather.6.cloned.1.call-done = bf16[1024,512]{1,0:T(8,128)(2,1)} async-done(((bf16[256,512]{1,0:T(8,128)(2,1)}), bf16[1024,512]{1,0:T(8,128)(2,1)}) %all-gather.6.cloned.1.call-update) | async-done | bytes 1048592 | tf_op jit(solution)/shard_map/all_gather | solution.py:40
  29.0 1.5 bitcast_convert_fusion
  30.6 1.4 copy.21
  31.9 0.0 copy-start.1
  31.9 0.0 copy-start.5
  31.9 0.9 copy.29
  32.8 0.3 copy-done.1
  33.1 0.3 multiply_reduce_fusion
  33.4 0.0 copy-done.5
  33.4 0.2 multiply_convert_fusion
  33.7 0.1 concatenate.11
  33.8 4.3 %gather_fusion = bf16[768,2048]{1,0:T(8,128)(2,1)} fusion(bf16[257,2048]{1,0:T(8,128)(2,1)S(1)} %concatenate.11, s32[1024]{0:T(1024)S(1)} %pad_clamp_fusion.1), kind=kCustom, calls=%fused_computation | custom fusion | bytes 6294528 | tf_op jit(solution)/shard_map/gather | solution.py:60
  38.1 1.2 constant_dynamic-slice_fusion
  39.3 25.9 %all_to_all.10 = bf16[8,1,24,2048]{3,2,1,0:T(8,128)(2,1)} all-to-all(bf16[8,1,24,2048]{3,2,1,0:T(8,128)(2,1)S(1)} %constant_dynamic-slice_fusion), channel_id=1, replica_groups=mesh['ep'=8,'tp'=4] {'ep'}, dimensions={0} | all-to-all | bytes 1572864 | tf_op jit(solution)/shard_map/all_to_all | solution.py:63
  65.2 0.0 all-gather.4.cloned.1.call-update
  65.2 0.0 reduce-scatter.5.cloned.1.call-start
  65.3 26.7 %all-gather.4.cloned.1.call-done = bf16[8,1,96,2048]{3,2,0,1:T(8,128)(2,1)} async-done(((bf16[8,1,24,2048]{3,2,0,1:T(8,128)(2,1)}), bf16[8,1,96,2048]{3,2,0,1:T(8,128)(2,1)}) %all-gather.4.cloned.1.call-update) | async-done | bytes 3145744 | tf_op jit(solution)/shard_map/all_gather | solution.py:64
  92.0 8.0 %fusion.4 = f32[8,96,896]{2,1,0:T(8,128)} fusion(bf16[1,2048,896]{2,1,0:T(8,128)(2,1)} %param.21, bf16[8,1,96,2048]{3,2,0,1:T(8,128)(2,1)} %all-gather.4.cloned.1.call-done), kind=kOutput, calls=%fused_computation.7 | convolution fusion | flops 2818572288 | bytes 9568256 | tf_op jit(solution)/shard_map/secd,edf->secf/dot_general | solution.py:65
  100.0 12.1 %fusion.11 = bf16[8,1,96,2048]{3,2,0,1:T(8,128)(2,1)} fusion(bf16[1,896,2048]{2,1,0:T(8,128)(2,1)} %param.23, bf16[1,2048,896]{2,1,0:T(8,128)(2,1)} %param.22, bf16[8,1,96,2048]{3,2,0,1:T(8,128)(2,1)} %all-gather.4.cloned.1.call-done, f32[8,96,896]{2,1,0:T(8,128)} %fusion.4), kind=kOutput, calls=%fused_computation.12 | convolution fusion | flops 5642846208 | bytes 16384000 | tf_op jit(solution)/shard_map/secf,efd->secd/dot_general | solution.py:68
  112.1 0.0 copy-start.2
  112.1 0.0 copy-start.3
  112.1 0.0 copy-start.6
  112.1 0.0 copy-start.4
  112.1 0.0 reduce-scatter.5.cloned.1.call-update
  112.1 0.0 copy-start.7
  112.1 0.0 reduce-scatter.3.cloned.1.call-start
  112.2 0.8 copy-done.2
  113.0 0.1 copy-done.3
  113.1 3.4 %collective-permute-start = (bf16[2,2,256]{2,1,0:T(2,128)(2,1)S(1)}, bf16[2,2,256]{2,1,0:T(2,128)(2,1)S(1)}, u32[]{:S(2)}, u32[]{:S(2)}) collective-permute-start(bf16[2,2,256]{2,1,0:T(2,128)(2,1)S(1)} %pad_maximum_fusion), channel_id=1, source_target_pairs={{0,4},{4,8},{8,12},{12,16},{16,20},{20,24},{24,28},{1,5},{5,9},{9,... | collective-permute-start | bytes 6152 | tf_op jit(solution)/shard_map/ppermute | solution.py:10
  116.5 0.0 copy-done.6
  116.5 1.3 collective-permute-done
  117.8 0.1 convert_multiply_fusion
  117.8 0.0 copy-done
  117.8 0.0 copy-done.4
  117.8 1.5 convolution_convert_fusion
  119.3 0.0 reduce-scatter.3.cloned.1.call-update
  119.3 30.7 %reduce-scatter.5.cloned.1.call-done = bf16[8,1,96,512]{3,2,0,1:T(8,128)(2,1)} async-done(((bf16[8,1,96,2048]{3,2,0,1:T(8,128)(2,1)}), bf16[8,1,96,512]{3,2,0,1:T(8,128)(2,1)}) %reduce-scatter.5.cloned.1.call-update) | async-done | bytes 786448 | tf_op jit(solution)/shard_map/reduce_scatter | solution.py:69
  150.0 5.5 %all-to-all-start.1 = ((bf16[8,1,96,512]{3,2,1,0:T(8,128)(2,1)}), bf16[8,1,96,512]{3,2,1,0:T(8,128)(2,1)S(1)}, u32[]{:S(2)}, u32[]{:S(2)}) async-start(bf16[8,1,96,512]{3,2,1,0:T(8,128)(2,1)} %bitcast.116), calls=%async_computation.3 | async-start | bytes 1572864 | tf_op jit(solution)/shard_map/all_to_all | solution.py:70
  155.5 0.0 copy-done.7
  155.5 0.1 copy.28
  155.7 19.9 %all-to-all-done.1 = bf16[8,1,96,512]{3,2,1,0:T(8,128)(2,1)S(1)} async-done(((bf16[8,1,96,512]{3,2,1,0:T(8,128)(2,1)}), bf16[8,1,96,512]{3,2,1,0:T(8,128)(2,1)S(1)}, u32[]{:S(2)}, u32[]{:S(2)}) %all-to-all-start.1) | async-done | bytes 786464 | tf_op jit(solution)/shard_map/all_to_all | solution.py:70
  175.6 2.0 %gather_fusion.1 = bf16[512,512]{1,0:T(8,128)(2,1)S(1)} fusion(bf16[768,512]{1,0:T(8,128)(2,1)S(1)} %bitcast.110, s32[1024]{0:T(1024)S(1)} %pad_clamp_fusion), kind=kCustom, calls=%fused_computation.1 | custom fusion | bytes 1050624 | tf_op jit(solution)/shard_map/gather | solution.py:72
  177.6 0.7 reshape.103
  178.2 2.1 %multiply_reduce_fusion.1 = bf16[256,512]{1,0:T(8,128)(2,1)} fusion(f32[256,2,512]{2,1,0:T(2,128)S(1)} %reshape.103, f32[256,2]{1,0:T(8,128)S(1)} %copy.28), kind=kLoop, calls=%fused_computation.24 | loop fusion | flops 393216 | bytes 1312768 | tf_op jit(solution)/shard_map/reduce_sum | solution.py:73
  180.3 0.0 reduce-scatter.3.cloned.1.call-done
  (13 shorter events, 0.1 us)
Async XLA Ops:
  7.2 110.7 %copy-start = (bf16[256,2048]{1,0:T(8,128)(2,1)S(1)}, bf16[256,2048]{1,0:T(8,128)(2,1)}, u32[]{:S(2)}) copy-start(bf16[256,2048]{1,0:T(8,128)(2,1)} %param.16) | copy-start | bytes 3145732
  7.2 21.9 %all-gather.6.cloned.1.call-start = ((), (), s32[]{:S(2)}) async-start(), calls=%async_computation.7 | async-start | bytes 1310720 | tf_op jit(solution)/shard_map/all_gather | solution.py:40
  7.9 84.1 %all-gather.4.cloned.1.call-start = ((), (), s32[]{:S(2)}) async-start(), calls=%async_computation.5 | async-start | bytes 3932160 | tf_op jit(solution)/shard_map/all_gather | solution.py:64
  31.9 1.2 copy-start.1
  31.9 1.5 copy-start.5
  65.2 84.8 %reduce-scatter.5.cloned.1.call-start = ((), (), s32[]{:S(2)}) async-start(), calls=%async_computation.6 | async-start | bytes 3932160 | tf_op jit(solution)/shard_map/reduce_scatter | solution.py:69
  112.1 0.9 copy-start.2
  112.1 1.0 copy-start.3
  112.1 4.4 %copy-start.6 = (f32[3,256]{1,0:T(4,128)S(1)}, f32[3,256]{1,0:T(4,128)}, u32[]{:S(2)}) copy-start(f32[3,256]{1,0:T(4,128)} %param.15) | copy-start | bytes 9220
  112.1 5.7 %copy-start.4 = (bf16[256,256]{1,0:T(8,128)(2,1)S(1)}, bf16[256,256]{1,0:T(8,128)(2,1)}, u32[]{:S(2)}) copy-start(bf16[256,256]{1,0:T(8,128)(2,1)} %param.12) | copy-start | bytes 393220
  112.1 43.4 %copy-start.7 = (f32[256,2]{0,1:T(2,128)S(1)}, f32[256,2]{0,1:T(2,128)}, u32[]{:S(2)}) copy-start(f32[256,2]{0,1:T(2,128)} %param.20) | copy-start | bytes 6148
  112.1 68.1 %reduce-scatter.3.cloned.1.call-start = ((), (), s32[]{:S(2)}) async-start(), calls=%async_computation.4 | async-start | bytes 1310720 | tf_op jit(solution)/shard_map/reduce_scatter | solution.py:31
  113.1 4.7 %collective-permute-start = (bf16[2,2,256]{2,1,0:T(2,128)(2,1)S(1)}, bf16[2,2,256]{2,1,0:T(2,128)(2,1)S(1)}, u32[]{:S(2)}, u32[]{:S(2)}) collective-permute-start(bf16[2,2,256]{2,1,0:T(2,128)(2,1)S(1)} %pad_maximum_fusion), channel_id=1, source_target_pairs={{0,4},{4,8},{8,12},{12,16},{16,20},{20,24},{24,28},{1,5},{5,9},{9,... | collective-permute-start | bytes 6152 | tf_op jit(solution)/shard_map/ppermute | solution.py:10
  150.0 25.6 %all-to-all-start.1 = ((bf16[8,1,96,512]{3,2,1,0:T(8,128)(2,1)}), bf16[8,1,96,512]{3,2,1,0:T(8,128)(2,1)S(1)}, u32[]{:S(2)}, u32[]{:S(2)}) async-start(bf16[8,1,96,512]{3,2,1,0:T(8,128)(2,1)} %bitcast.116), calls=%async_computation.3 | async-start | bytes 1572864 | tf_op jit(solution)/shard_map/all_to_all | solution.py:70
Sparse Core Ops, SparseCore 0:
  9.5 19.4 all-gather.5
  65.4 26.6 all-gather.3
  112.3 37.7 reduce-scatter.4
  153.0 24.8 reduce-scatter.2
